TPU v7x, 32 devices: a whole 2x2x4 slice. The times are simulated.
32 devices in a mesh: sp: 8 (over z, x), dp: 4 (over y, core).
Axes of the slice: x: 2, y: 2, z: 4, core: 2. Of those that a mesh axis runs over, the one named last changes fastest.
Arguments:
- hidden_in: bfloat16 [4, 1024, 2048], P('dp', 'sp'), may hold values from -6 to 6
- mix_cotangent: bfloat16 [4, 1024, 4096], P('dp', 'sp'), may hold values from -0.119628906 to 0.119628906
- query_weight: bfloat16 [2048, 4096], P('dp', 'sp'), may hold values from -0.125 to 0.125
- key_weight: bfloat16 [2048, 4096], P('dp', 'sp'), may hold values from -0.125 to 0.125
- value_weight: bfloat16 [2048, 4096], P('dp', 'sp'), may hold values from -0.125 to 0.125
- decay_log: float32 [16], P('sp'), may hold values from -0.034 to -0.00029296875, as said below
Outputs:
- grad_hidden: bfloat16 [4, 1024, 2048], P('dp', 'sp')
- grad_query: float32 [2048, 4096], P('dp', 'sp')
- grad_key: float32 [2048, 4096], P('dp', 'sp')
- grad_value: float32 [2048, 4096], P('dp', 'sp')
Inputs may be any that keep to these rules, and one draw needn't show every extreme that they name: Each head's decay_log is negative.
All inputs are finite; a program needn't handle non-finite values.
Results may differ from a plain program's by a relative error of at most 0.015.
Values may be sent and summed in bfloat16 or wider, within the bound.
A program may use at most 64 MiB of HBM per device.

v0:
```python
import jax
import jax.numpy as jnp
from jax import lax
from jax.sharding import PartitionSpec as P

BLOCK = 128


def head_grads(queries, key_rows, values, cotangent, log_rate):
    length = queries.shape[0]
    head_dim = queries.shape[1]
    blocks = length // BLOCK
    scale = head_dim ** (-0.5)
    keys_scaled = (key_rows.astype(jnp.float32) * scale).astype(jnp.bfloat16)
    offsets = jnp.arange(BLOCK, dtype=jnp.float32)
    spread = offsets[:, None] - offsets[None, :]
    inner_decay = jnp.where(spread >= 0, jnp.exp(log_rate * jnp.maximum(spread, 0.0)), 0.0)
    query_decay = jnp.exp(log_rate * (offsets + 1.0))
    key_decay = jnp.exp(log_rate * (BLOCK - 1.0 - offsets))
    block_decay = jnp.exp(log_rate * BLOCK)

    def split_blocks(series):
        return series.reshape(blocks, BLOCK, series.shape[-1])

    def forward(carried, inputs):
        query_block, key_block, value_block, grad_block = inputs
        mixed = (
            jnp.dot(grad_block, value_block.T, preferred_element_type=jnp.float32) * inner_decay
        ).astype(jnp.bfloat16)
        within = jnp.dot(mixed, key_block, preferred_element_type=jnp.float32)
        across = (
            jnp.dot(grad_block, carried.astype(jnp.bfloat16).T, preferred_element_type=jnp.float32)
            * query_decay[:, None]
        )
        weighted = (key_block.astype(jnp.float32) * key_decay[:, None]).astype(jnp.bfloat16)
        updated = carried * block_decay + jnp.dot(
            weighted.T, value_block, preferred_element_type=jnp.float32
        )
        return (updated, (within + across, mixed))

    def backward(carried, inputs):
        query_block, key_block, value_block, grad_block, mixed = inputs
        scores = (
            jnp.dot(query_block, key_block.T, preferred_element_type=jnp.float32) * inner_decay
        ).astype(jnp.bfloat16)
        state_bf = carried.astype(jnp.bfloat16)
        grad_v = (
            jnp.dot(scores.T, grad_block, preferred_element_type=jnp.float32)
            + jnp.dot(key_block, state_bf, preferred_element_type=jnp.float32) * key_decay[:, None]
        )
        grad_k = (
            jnp.dot(mixed.T, query_block, preferred_element_type=jnp.float32)
            + jnp.dot(value_block, state_bf.T, preferred_element_type=jnp.float32)
            * key_decay[:, None]
        ) * scale
        weighted = (query_block.astype(jnp.float32) * query_decay[:, None]).astype(jnp.bfloat16)
        updated = carried * block_decay + jnp.dot(
            weighted.T, grad_block, preferred_element_type=jnp.float32
        )
        return (updated, (grad_k, grad_v))

    inputs = (
        split_blocks(queries),
        split_blocks(keys_scaled),
        split_blocks(values),
        split_blocks(cotangent),
    )
    initial = jnp.zeros((head_dim, values.shape[-1]), jnp.float32)
    final_state, (grad_q, mixed_all) = lax.scan(forward, initial, inputs)
    final_back, (grad_k, grad_v) = lax.scan(backward, initial, inputs + (mixed_all,), reverse=True)
    return (grad_q.reshape(length, -1), grad_k.reshape(length, -1), grad_v.reshape(length, -1))


def group_grads(log_rates, queries, key_rows, values, cotangent):
    length = queries.shape[0]
    head_count = log_rates.shape[0]

    def by_head(series):
        return series.reshape(length, head_count, -1).transpose(1, 0, 2)

    def to_rows(series):
        return series.transpose(1, 0, 2).reshape(length, -1)

    grad_q, grad_k, grad_v = jax.vmap(head_grads)(
        by_head(queries), by_head(key_rows), by_head(values), by_head(cotangent), log_rates
    )
    return jnp.concatenate((to_rows(grad_q), to_rows(grad_k), to_rows(grad_v)), axis=1).astype(
        jnp.bfloat16
    )


def body(hidden_in, mix_cotangent, query_weight, key_weight, value_weight, decay_log):
    own_rows = hidden_in[0]
    columns = query_weight.shape[1]
    stacked = jnp.stack((query_weight, key_weight, value_weight), axis=1)
    gathered = lax.all_gather(stacked, "dp", axis=0, tiled=True)
    weights = gathered.reshape(gathered.shape[0], 3 * columns)
    cotangent = lax.all_to_all(mix_cotangent[0], "sp", split_axis=1, concat_axis=0, tiled=True)
    all_rows = lax.all_gather(own_rows, "sp", axis=0, tiled=True)
    projected = jnp.dot(all_rows, weights, preferred_element_type=jnp.float32).astype(jnp.bfloat16)
    gradients = group_grads(
        decay_log,
        projected[:, :columns],
        projected[:, columns : 2 * columns],
        projected[:, 2 * columns :],
        cotangent,
    )
    input_sum = lax.psum_scatter(
        lax.dot_general(
            gradients, weights, (((1,), (1,)), ((), ())), preferred_element_type=jnp.float32
        ).astype(jnp.bfloat16),
        "sp",
        scatter_dimension=0,
        tiled=True,
    )
    grad_hidden = input_sum[None]
    summed = lax.psum_scatter(
        lax.dot_general(
            all_rows, gradients, (((0,), (0,)), ((), ())), preferred_element_type=jnp.float32
        ).astype(jnp.bfloat16),
        "dp",
        scatter_dimension=0,
        tiled=True,
    ).astype(jnp.float32) / lax.axis_size("dp")
    return (
        grad_hidden,
        summed[:, :columns],
        summed[:, columns : 2 * columns],
        summed[:, 2 * columns :],
    )


def solution(mesh):
    placed = (
        P("dp", "sp", None),
        P("dp", "sp", None),
        P("dp", "sp"),
        P("dp", "sp"),
        P("dp", "sp"),
        P("sp"),
    )
    return jax.shard_map(
        body,
        mesh=mesh,
        in_specs=placed,
        out_specs=(P("dp", "sp", None), P("dp", "sp"), P("dp", "sp"), P("dp", "sp")),
        check_vma=False,
    )
```

profile of v0, /device:TPU:0, one launch (start us, length us, event | category | flops | bytes accessed | tf_op | source)
XLA Modules:
  0.0 433.3 jit_solution(4035622993823633458)
XLA Ops:
  14.4 7.3 %all-to-all-start = ((bf16[128,8,512]{0,2,1:T(8,128)(2,1)}), bf16[128,8,512]{0,2,1:T(8,128)(2,1)S(1)}, u32[]{:S(2)}, u32[]{:S(2)}) async-start(bf16[128,8,512]{0,2,1:T(8,128)(2,1)} %bitcast.14), calls=%async_computation | async-start | bytes 2097152 | tf_op jit(solution)/shard_map/all_to_all | solution.py:98
  21.9 42.4 %all-to-all-done = bf16[128,8,512]{0,2,1:T(8,128)(2,1)S(1)} async-done(((bf16[128,8,512]{0,2,1:T(8,128)(2,1)}), bf16[128,8,512]{0,2,1:T(8,128)(2,1)S(1)}, u32[]{:S(2)}, u32[]{:S(2)}) %all-to-all-start) | async-done | bytes 1048608 | tf_op jit(solution)/shard_map/all_to_all | solution.py:98
  66.1 39.1 %all-gather.6.cloned.1.call-done = bf16[1,1024,2048]{2,1,0:T(8,128)(2,1)} async-done(((bf16[1,128,2048]{2,1,0:T(8,128)(2,1)}), bf16[1,1024,2048]{2,1,0:T(8,128)(2,1)}) %all-gather.6.cloned.1.call-update) | async-done | bytes 4194320 | tf_op jit(solution)/shard_map/all_gather | solution.py:99
  105.1 46.5 %all-gather.4.cloned.1.call-done = bf16[2048,3,512]{0,2,1:T(8,128)(2,1)} async-done(((bf16[512,3,512]{0,2,1:T(8,128)(2,1)}), bf16[2048,3,512]{0,2,1:T(8,128)(2,1)}) %all-gather.4.cloned.1.call-update) | async-done | bytes 6291472 | tf_op jit(solution)/shard_map/all_gather | solution.py:96
  151.6 10.1 %fusion.93 = bf16[1024,1536]{0,1:T(8,128)(2,1)S(1)} fusion(bf16[2048,1536]{0,1:T(8,128)(2,1)} %bitcast.197, bf16[1,1024,2048]{2,1,0:T(8,128)(2,1)} %all-gather.6.cloned.1.call-done), kind=kOutput, calls=%fused_computation.98 | convolution fusion | flops 6444023808 | bytes 13631488 | tf_op jit(solution)/shard_map/dot_general | solution.py:100
  163.4 2.3 copy.54
  165.6 2.3 copy.59
  171.6 33.4 %while.38 = (s32[]{:T(128)}, f32[2,256,256]{2,1,0:T(8,128)S(1)}, bf16[8,2,128,256]{3,2,0,1:T(8,128)(2,1)}, bf16[8,2,128,128]{3,2,1,0:T(8,128)(2,1)}, f32[2]{0:T(...) while((s32[]{:T(128)}, f32[2,256,256]{2,1,0:T(8,128)S(1)}, ...), condition=%wide.region_1.2_spmd.clone.clone.clone, body=%wide.region_0.1_spmd.clone.clone.clone.sunk | while | flops 101646848 | bytes 3434148 | solution.py:69
  171.6 1.7 bitcast_dynamic-update-slice_fusion.2
  175.8 1.7 bitcast_dynamic-update-slice_fusion.2
  179.9 1.7 bitcast_dynamic-update-slice_fusion.2
  184.1 1.7 bitcast_dynamic-update-slice_fusion.2
  188.3 1.7 bitcast_dynamic-update-slice_fusion.2
  192.5 1.7 bitcast_dynamic-update-slice_fusion.2
  196.7 1.7 bitcast_dynamic-update-slice_fusion.2
  200.8 1.7 bitcast_dynamic-update-slice_fusion.2
  205.0 2.3 copy.63
  209.4 52.0 %while.39 = (s32[]{:T(128)}, f32[2,256,256]{2,1,0:T(8,128)S(1)}, bf16[8,2,128,256]{3,2,0,1:T(8,128)(2,1)}, bf16[8,2,128,256]{3,2,0,1:T(8,128)(2,1)}, f32[2]{0:T(...) while((s32[]{:T(128)}, f32[2,256,256]{2,1,0:T(8,128)S(1)}, ...), condition=%wide.region_3.4_spmd.clone.clone.clone, body=%wide.region_2.3_spmd.clone.clone.clone.sunk | while | flops 152306176 | bytes 4880578 | solution.py:70
  212.8 1.8 fusion.138
  219.3 1.8 fusion.138
  225.8 1.8 fusion.138
  232.3 1.8 fusion.138
  238.8 1.8 fusion.138
  245.4 1.8 fusion.138
  251.9 1.8 fusion.138
  258.4 1.8 fusion.138
  261.4 1.6 copy.70
  265.9 10.4 %fusion.86 = bf16[2048,1536]{0,1:T(8,128)(2,1)} fusion(bf16[1,1024,2048]{2,1,0:T(8,128)(2,1)} %all-gather.6.cloned.1.call-done, bf16[1024,512]{0,1:T(8,128)(2,1)S(1)} %bitcast.193, bf16[1024,512]{0,1:T(8,128)(2,1)S(1)} %bitcast.191, bf16[1024,512]{0,1:T(8,128)(2,1)} %bitcast.195), kind=kOutput, calls=%fused_computation.92 | convolution fusion | flops 6455033856 | bytes 13631488 | tf_op jit(solution)/shard_map/dot_general | solution.py:118
  277.5 11.1 %convolution_convert_fusion.1 = bf16[1024,2048]{1,0:T(8,128)(2,1)} fusion(bf16[2048,1536]{0,1:T(8,128)(2,1)} %bitcast.198, bf16[1024,512]{0,1:T(8,128)(2,1)S(1)} %bitcast.194, bf16[1024,512]{0,1:T(8,128)(2,1)S(1)} %bitcast.192, bf16[1024,512]{0,1:T(8,128)(2,1)S(1)} %bitcast.196), kind=kOutput, calls=%fused_computation.96 | convolution fusion | flops 6453985280 | bytes 13631488 | tf_op jit(solution)/shard_map/dot_general | solution.py:109
  288.7 45.7 %reduce-scatter.5.cloned.1.call-done = bf16[512,1536]{0,1:T(8,128)(2,1)} async-done(((bf16[2048,1536]{0,1:T(8,128)(2,1)}), bf16[512,1536]{0,1:T(8,128)(2,1)}) %reduce-scatter.5.cloned.1.call-update) | async-done | bytes 1572880 | tf_op jit(solution)/shard_map/reduce_scatter | solution.py:117
  334.3 1.8 convert_multiply_fusion
  340.4 86.3 %reduce-scatter.3.cloned.1.call-done = bf16[128,2048]{1,0:T(8,128)(2,1)} async-done(((bf16[1024,2048]{1,0:T(8,128)(2,1)}), bf16[128,2048]{1,0:T(8,128)(2,1)}) %reduce-scatter.3.cloned.1.call-update) | async-done | bytes 524304 | tf_op jit(solution)/shard_map/reduce_scatter | solution.py:108
  (117 shorter events, 81.4 us)
Async XLA Ops:
  7.2 5.9 %copy-start.1 = (bf16[1,128,4096]{2,1,0:T(8,128)(2,1)S(1)}, bf16[1,128,4096]{2,1,0:T(8,128)(2,1)}, u32[]{:S(2)}) copy-start(bf16[1,128,4096]{2,1,0:T(8,128)(2,1)} %param.11) | copy-start | bytes 3145732
  7.2 98.0 %all-gather.6.cloned.1.call-start = ((), (), s32[]{:S(2)}) async-start(), calls=%async_computation.6 | async-start | bytes 4718592 | tf_op jit(solution)/shard_map/all_gather | solution.py:99
  7.9 143.7 %all-gather.4.cloned.1.call-start = ((), (), s32[]{:S(2)}) async-start(), calls=%async_computation.3 | async-start | bytes 7864320 | tf_op jit(solution)/shard_map/all_gather | solution.py:96
  11.7 10.1 %copy-start.3 = (f32[2]{0:T(128)S(1)}, f32[2]{0:T(128)}, u32[]{:S(2)}) copy-start(f32[2]{0:T(128)} %param.15) | copy-start | bytes 28
  14.4 49.9 %all-to-all-start = ((bf16[128,8,512]{0,2,1:T(8,128)(2,1)}), bf16[128,8,512]{0,2,1:T(8,128)(2,1)S(1)}, u32[]{:S(2)}, u32[]{:S(2)}) async-start(bf16[128,8,512]{0,2,1:T(8,128)(2,1)} %bitcast.14), calls=%async_computation | async-start | bytes 2097152 | tf_op jit(solution)/shard_map/all_to_all | solution.py:98
  21.7 312.7 %reduce-scatter.5.cloned.1.call-start = ((), (), s32[]{:S(2)}) async-start(), calls=%async_computation.5 | async-start | bytes 7864320 | tf_op jit(solution)/shard_map/reduce_scatter | solution.py:117
  261.4 3.1 copy-start
  276.3 1.2 copy-start.2
  276.3 150.4 %reduce-scatter.3.cloned.1.call-start = ((), (), s32[]{:S(2)}) async-start(), calls=%async_computation.4 | async-start | bytes 4718592 | tf_op jit(solution)/shard_map/reduce_scatter | solution.py:108
Sparse Core Ops, SparseCore 0:
  10.1 94.9 all-gather.5
  106.7 44.8 all-gather.3
  276.4 57.8 reduce-scatter.4
  338.4 88.2 reduce-scatter.2
where the time goes:
time: 435 us; the launch traced here: 433 us
  waiting for transfers between devices  261 us (60%)
  matrix products  115 us (26%)
  local copies, waits for them, and re-layouts  30.6 us (7%)
  between operations  14 us (3%)
  starting transfers between devices  7.62 us (2%)
  other arithmetic  4.64 us (1%)
    reduce_scatter x1, waiting for transfers between devices, body(): lax.psum_scatter(lax.dot_general(gradients, weights, (((1,), (1,)), ((),...  86.3 us
    all_gather x1, waiting for transfers between devices, body(): gathered = lax.all_gather(stacked, 'dp', axis=0, tiled=True)  46.5 us
    reduce_scatter x1, waiting for transfers between devices, body(): lax.psum_scatter(lax.dot_general(all_rows, gradients, (((0,), (0,)), ((),...  45.7 us
    all_to_all x1, waiting for transfers between devices, body(): lax.all_to_all(mix_cotangent[0], 'sp', split_axis=1, concat_axis=0, tiled...  42.4 us
    all_gather x1, waiting for transfers between devices, body(): all_rows = lax.all_gather(own_rows, 'sp', axis=0, tiled=True)  39.1 us
    dot_general x8, matrix products, backward(): jnp.dot(value_block, state_bf.T, preferred_element_type=jnp.float32)  14.4 us
    dot_general x8, matrix products, forward(): jnp.dot(grad_block, value_block.T, preferred_element_type=jnp.float32)  13.9 us
    unnamed x18, local copies, waits for them, and re-layouts  13.7 us
  transfers between devices with their start and end apart: 5, of which 5 were waited for; matrix products, arithmetic and copies ran while one was open for 6% of the time, Pallas kernels for 0%

commit v1 on v0

--- a/solution.py
+++ b/solution.py
@@ -93,7 +93,12 @@
     own_rows = hidden_in[0]
     columns = query_weight.shape[1]
     stacked = jnp.stack((query_weight, key_weight, value_weight), axis=1)
-    gathered = lax.all_gather(stacked, "dp", axis=0, tiled=True)
+    ring = [stacked]
+    for hop in range(3):
+        ring.append(lax.ppermute(ring[-1], "dp", [(dev, (dev + 1) % 4) for dev in range(4)]))
+    gathered = jnp.roll(
+        jnp.concatenate(ring[::-1], axis=0), (lax.axis_index("dp") + 1) * ring[0].shape[0], axis=0
+    )
     weights = gathered.reshape(gathered.shape[0], 3 * columns)
     cotangent = lax.all_to_all(mix_cotangent[0], "sp", split_axis=1, concat_axis=0, tiled=True)
     all_rows = lax.all_gather(own_rows, "sp", axis=0, tiled=True)

time: 435 us -> 396 us (0.910)
  waiting for transfers between devices: 261 us -> 205 us
  local copies, waits for them, and re-layouts: 30.6 us -> 48.5 us
    all_gather x1 -> x0, waiting for transfers between devices: 46.5 us -> none  [body(): gathered = lax.all_gather(stacked, 'dp', axis=0, tiled=True)]
    all_gather x1, waiting for transfers between devices: 39.1 us -> 0.01 us  [body(): all_rows = lax.all_gather(own_rows, 'sp', axis=0, tiled=True)]
    ppermute x0 -> x3, waiting for transfers between devices: none -> 32.4 us  [body(): lax.ppermute(ring[-1], 'dp', [(dev, (dev + 1) % 4) for dev in range(4)])]
    unnamed x18 -> x28, local copies, waits for them, and re-layouts: 13.7 us -> 25 us
    all_to_all x1, waiting for transfers between devices: 42.4 us -> 34.9 us  [body(): lax.all_to_all(mix_cotangent[0], 'sp', split_axis=1, concat_axis=0, tiled...]
    reduce_scatter x1, waiting for transfers between devices: 45.7 us -> 50.2 us  [body(): lax.psum_scatter(lax.dot_general(all_rows, gradients, (((0,), (0,)), ((),...]
  transfers between devices with their start and end apart: 5 -> 7, of which waited for: 5 -> 5; matrix products, arithmetic and copies ran while one was open for 6% -> 11% of each run, Pallas kernels for 0% -> 0%
where the time goes in v1:
time: 396 us; the launch traced here: 394 us
  waiting for transfers between devices  205 us (52%)
  matrix products  115 us (29%)
  local copies, waits for them, and re-layouts  48.5 us (12%)
  between operations  14 us (4%)
  starting transfers between devices  7.25 us (2%)
  other arithmetic  3.96 us (1%)
    reduce_scatter x1, waiting for transfers between devices, body(): lax.psum_scatter(lax.dot_general(gradients, weights, (((1,), (1,)), ((),...  86.4 us
    reduce_scatter x1, waiting for transfers between devices, body(): lax.psum_scatter(lax.dot_general(all_rows, gradients, (((0,), (0,)), ((),...  50.2 us
    all_to_all x1, waiting for transfers between devices, body(): lax.all_to_all(mix_cotangent[0], 'sp', split_axis=1, concat_axis=0, tiled...  34.9 us
    ppermute x3, waiting for transfers between devices, body(): lax.ppermute(ring[-1], 'dp', [(dev, (dev + 1) % 4) for dev in range(4)])  32.4 us
    unnamed x28, local copies, waits for them, and re-layouts  25 us
    dot_general x8, matrix products, backward(): jnp.dot(value_block, state_bf.T, preferred_element_type=jnp.float32)  14.4 us
    dot_general x8, matrix products, forward(): jnp.dot(grad_block, value_block.T, preferred_element_type=jnp.float32)  13.9 us
    dot_general x1, matrix products, body(): lax.dot_general(gradients, weights, (((1,), (1,)), ((), ())), preferred_e...  11.1 us
  transfers between devices with their start and end apart: 7, of which 5 were waited for; matrix products, arithmetic and copies ran while one was open for 11% of the time, Pallas kernels for 0%

profile of v1, /device:TPU:0, one launch (start us, length us, event | category | flops | bytes accessed | tf_op | source)
XLA Modules:
  0.0 394.3 jit_solution(9738966738681231560)
XLA Ops:
  12.4 20.1 %collective-permute-done = bf16[512,3,512]{0,2,1:T(8,128)(2,1)} collective-permute-done((bf16[512,3,512]{0,2,1:T(8,128)(2,1)S(1)}, bf16[512,3,512]{0,2,1:T(8,128)(2,1)}, u32[]{:S(2)}, u32[]{:S(2)}) %collective-permute-start) | collective-permute-done | bytes 1572896 | tf_op jit(solution)/shard_map/ppermute | solution.py:98
  33.9 6.6 %all-to-all-start = ((bf16[128,8,512]{0,2,1:T(8,128)(2,1)}), bf16[128,8,512]{0,2,1:T(8,128)(2,1)S(1)}, u32[]{:S(2)}, u32[]{:S(2)}) async-start(bf16[128,8,512]{0,2,1:T(8,128)(2,1)} %bitcast.189), calls=%async_computation | async-start | bytes 2097152 | tf_op jit(solution)/shard_map/all_to_all | solution.py:103
  40.5 12.2 %collective-permute-done.1 = bf16[512,3,512]{0,2,1:T(8,128)(2,1)} collective-permute-done((bf16[512,3,512]{0,2,1:T(8,128)(2,1)}, bf16[512,3,512]{0,2,1:T(8,128)(2,1)}, u32[]{:S(2)}, u32[]{:S(2)}) %collective-permute-start.1) | collective-permute-done | bytes 1572896 | tf_op jit(solution)/shard_map/ppermute | solution.py:98
  52.9 34.9 %all-to-all-done = bf16[128,8,512]{0,2,1:T(8,128)(2,1)S(1)} async-done(((bf16[128,8,512]{0,2,1:T(8,128)(2,1)}), bf16[128,8,512]{0,2,1:T(8,128)(2,1)S(1)}, u32[]{:S(2)}, u32[]{:S(2)}) %all-to-all-start) | async-done | bytes 1048608 | tf_op jit(solution)/shard_map/all_to_all | solution.py:103
  104.1 3.8 constant_dynamic-slice_fusion
  107.9 10.1 %fusion.93 = bf16[1024,1536]{0,1:T(8,128)(2,1)S(1)} fusion(bf16[2048,1536]{0,1:T(8,128)(2,1)} %bitcast.186, bf16[1,1024,2048]{2,1,0:T(8,128)(2,1)} %all-gather.3.cloned.1.call-done), kind=kOutput, calls=%fused_computation.98 | convolution fusion | flops 6444023808 | bytes 13631488 | tf_op jit(solution)/shard_map/dot_general | solution.py:105
  119.7 2.3 copy.63
  124.6 2.3 copy.54
  126.8 2.3 copy.59
  130.2 33.4 %while.38 = (s32[]{:T(128)}, f32[2,256,256]{2,1,0:T(8,128)S(1)}, bf16[8,2,128,256]{3,2,0,1:T(8,128)(2,1)}, bf16[8,2,128,128]{3,2,1,0:T(8,128)(2,1)}, f32[2]{0:T(...) while((s32[]{:T(128)}, f32[2,256,256]{2,1,0:T(8,128)S(1)}, ...), condition=%wide.region_1.2_spmd.clone.clone.clone, body=%wide.region_0.1_spmd.clone.clone.clone.sunk | while | flops 101646848 | bytes 3435178 | solution.py:69
  130.2 1.7 bitcast_dynamic-update-slice_fusion.2
  134.4 1.7 bitcast_dynamic-update-slice_fusion.2
  138.5 1.7 bitcast_dynamic-update-slice_fusion.2
  142.7 1.7 bitcast_dynamic-update-slice_fusion.2
  146.9 1.7 bitcast_dynamic-update-slice_fusion.2
  151.1 1.7 bitcast_dynamic-update-slice_fusion.2
  155.3 1.7 bitcast_dynamic-update-slice_fusion.2
  159.4 1.7 bitcast_dynamic-update-slice_fusion.2
  165.8 52.0 %while.39 = (s32[]{:T(128)}, f32[2,256,256]{2,1,0:T(8,128)S(1)}, bf16[8,2,128,256]{3,2,0,1:T(8,128)(2,1)}, bf16[8,2,128,256]{3,2,0,1:T(8,128)(2,1)}, f32[2]{0:T(...) while((s32[]{:T(128)}, f32[2,256,256]{2,1,0:T(8,128)S(1)}, ...), condition=%wide.region_3.4_spmd.clone.clone.clone, body=%wide.region_2.3_spmd.clone.clone.clone.sunk | while | flops 152306176 | bytes 4880586 | solution.py:70
  169.2 1.8 fusion.138
  175.7 1.8 fusion.138
  182.2 1.8 fusion.138
  188.7 1.8 fusion.138
  195.2 1.8 fusion.138
  201.7 1.8 fusion.138
  208.2 1.8 fusion.138
  214.7 1.8 fusion.138
  222.2 10.5 %fusion.86 = bf16[2048,1536]{0,1:T(8,128)(2,1)} fusion(bf16[1,1024,2048]{2,1,0:T(8,128)(2,1)} %all-gather.3.cloned.1.call-done, bf16[1024,512]{0,1:T(8,128)(2,1)S(1)} %bitcast.200, bf16[1024,512]{0,1:T(8,128)(2,1)S(1)} %bitcast.202, bf16[1024,512]{0,1:T(8,128)(2,1)} %bitcast.204), kind=kOutput, calls=%fused_computation.92 | convolution fusion | flops 6455033856 | bytes 13631488 | tf_op jit(solution)/shard_map/dot_general | solution.py:123
  233.8 11.1 %convolution_convert_fusion.1 = bf16[1024,2048]{1,0:T(8,128)(2,1)} fusion(bf16[2048,1536]{0,1:T(8,128)(2,1)} %bitcast.187, bf16[1024,512]{0,1:T(8,128)(2,1)S(1)} %bitcast.201, bf16[1024,512]{0,1:T(8,128)(2,1)S(1)} %bitcast.203, bf16[1024,512]{0,1:T(8,128)(2,1)S(1)} %bitcast.205), kind=kOutput, calls=%fused_computation.96 | convolution fusion | flops 6453985280 | bytes 13631488 | tf_op jit(solution)/shard_map/dot_general | solution.py:114
  245.0 50.2 %reduce-scatter.5.cloned.1.call-done = bf16[512,1536]{0,1:T(8,128)(2,1)} async-done(((bf16[2048,1536]{0,1:T(8,128)(2,1)}), bf16[512,1536]{0,1:T(8,128)(2,1)}) %reduce-scatter.5.cloned.1.call-update) | async-done | bytes 1572880 | tf_op jit(solution)/shard_map/reduce_scatter | solution.py:122
  295.2 1.8 convert_multiply_fusion
  301.3 86.4 %reduce-scatter.3.cloned.1.call-done = bf16[128,2048]{1,0:T(8,128)(2,1)} async-done(((bf16[1024,2048]{1,0:T(8,128)(2,1)}), bf16[128,2048]{1,0:T(8,128)(2,1)}) %reduce-scatter.3.cloned.1.call-update) | async-done | bytes 524304 | tf_op jit(solution)/shard_map/reduce_scatter | solution.py:113
  (133 shorter events, 96.7 us)
Async XLA Ops:
  7.2 25.4 %copy-start.3 = (bf16[1,128,4096]{2,1,0:T(8,128)(2,1)S(1)}, bf16[1,128,4096]{2,1,0:T(8,128)(2,1)}, u32[]{:S(2)}) copy-start(bf16[1,128,4096]{2,1,0:T(8,128)(2,1)} %param.11) | copy-start | bytes 3145732
  7.2 100.7 %all-gather.3.cloned.1.call-start = ((), (), s32[]{:S(2)}) async-start(), calls=%async_computation.5 | async-start | bytes 4718592 | tf_op jit(solution)/shard_map/all_gather | solution.py:104
  10.4 42.4 %copy-start.5 = (f32[2]{0:T(128)S(1)}, f32[2]{0:T(128)}, u32[]{:S(2)}) copy-start(f32[2]{0:T(128)} %param.15) | copy-start | bytes 28
  11.7 41.1 %copy-start = (bf16[512,512]{0,1:T(8,128)(2,1)}, bf16[512,512]{0,1:T(8,128)(2,1)S(1)}, u32[]{:S(2)}) copy-start(bf16[512,512]{0,1:T(8,128)(2,1)S(1)} %copy.50) | copy-start | bytes 1572868
  11.9 20.7 %collective-permute-start = (bf16[512,3,512]{0,2,1:T(8,128)(2,1)S(1)}, bf16[512,3,512]{0,2,1:T(8,128)(2,1)}, u32[]{:S(2)}, u32[]{:S(2)}) collective-permute-start(bf16[512,3,512]{0,2,1:T(8,128)(2,1)S(1)} %pad_maximum_fusion.1), channel_id=1, source_target_pairs={{0,1},{1,2},{2,3},{3,0},{4,5},{5,6},{6,7},{7,4},{8,9},{9,10},{10,1... | collective-permute-start | bytes 4718600 | tf_op jit(solution)/shard_map/ppermute | solution.py:98
  32.6 20.2 %collective-permute-start.1 = (bf16[512,3,512]{0,2,1:T(8,128)(2,1)}, bf16[512,3,512]{0,2,1:T(8,128)(2,1)}, u32[]{:S(2)}, u32[]{:S(2)}) collective-permute-start(bf16[512,3,512]{0,2,1:T(8,128)(2,1)} %collective-permute-done), channel_id=1, source_target_pairs={{0,1},{1,2},{2,3},{3,0},{4,5},{5,6},{6,7},{7,4},{8,9},{9,10},{10,1... | collective-permute-start | bytes 4718600 | tf_op jit(solution)/shard_map/ppermute | solution.py:98
  33.9 53.9 %all-to-all-start = ((bf16[128,8,512]{0,2,1:T(8,128)(2,1)}), bf16[128,8,512]{0,2,1:T(8,128)(2,1)S(1)}, u32[]{:S(2)}, u32[]{:S(2)}) async-start(bf16[128,8,512]{0,2,1:T(8,128)(2,1)} %bitcast.189), calls=%async_computation | async-start | bytes 2097152 | tf_op jit(solution)/shard_map/all_to_all | solution.py:103
  40.5 254.7 %reduce-scatter.5.cloned.1.call-start = ((), (), s32[]{:S(2)}) async-start(), calls=%async_computation.4 | async-start | bytes 7864320 | tf_op jit(solution)/shard_map/reduce_scatter | solution.py:122
  52.8 40.9 %collective-permute-start.2 = (bf16[512,3,512]{0,2,1:T(8,128)(2,1)}, bf16[512,3,512]{0,2,1:T(8,128)(2,1)}, u32[]{:S(2)}, u32[]{:S(2)}) collective-permute-start(bf16[512,3,512]{0,2,1:T(8,128)(2,1)} %collective-permute-done.1), channel_id=1, source_target_pairs={{0,1},{1,2},{2,3},{3,0},{4,5},{5,6},{6,7},{7,4},{8,9},{9,10},{10,1... | collective-permute-start | bytes 4718600 | tf_op jit(solution)/shard_map/ppermute | solution.py:98
  93.6 5.1 %copy-start.1 = (bf16[512,512]{0,1:T(8,128)(2,1)S(1)}, bf16[512,512]{0,1:T(8,128)(2,1)}, u32[]{:S(2)}) copy-start(bf16[512,512]{0,1:T(8,128)(2,1)} %copy-done) | copy-start | bytes 1572868
  217.7 3.1 copy-start.2
  232.6 1.2 copy-start.4
  232.6 155.1 %reduce-scatter.3.cloned.1.call-start = ((), (), s32[]{:S(2)}) async-start(), calls=%async_computation.3 | async-start | bytes 4718592 | tf_op jit(solution)/shard_map/reduce_scatter | solution.py:113
Sparse Core Ops, SparseCore 0:
  10.1 92.2 all-gather.2
  232.8 62.4 reduce-scatter.4
  299.4 88.2 reduce-scatter.2
